TPU v7x, 32 devices: a whole 2x2x4 slice. The times are simulated.
32 devices in a mesh: sp: 8 (over z, x), tp: 4 (over y, core).
Axes of the slice: x: 2, y: 2, z: 4, core: 2. Of those that a mesh axis runs over, the one named last changes fastest.
Arguments:
- tokens: bfloat16 [1024, 1024], P('sp', 'tp'), may hold values from -6 to 6
- norm_gain: float32 [3, 1024], replicated, may hold values from 0.1 to 1.9
- w_query: bfloat16 [3, 1024, 1024], P(None, 'sp', 'tp'), may hold values from -0.1875 to 0.1875
- w_key: bfloat16 [3, 1024, 1024], P(None, 'sp', 'tp'), may hold values from -0.1875 to 0.1875
- w_value: bfloat16 [3, 1024, 1024], P(None, 'sp', 'tp'), may hold values from -0.1875 to 0.1875
- w_out: bfloat16 [3, 1024, 1024], P(None, 'tp', 'sp'), may hold values from -0.5625 to 0.5625
- offset_bias: float32 [3, 16, 8, 16], P(None, 'tp'), may hold values from -3 to 3
- documents: int32 [1024], P('sp'), may hold values from 0 to 7, never falling along the last dimension, each value on 1 to 256 neighbouring positions
Outputs:
- mixed: bfloat16 [1024, 1024], P('sp', 'tp')
Inputs may be any that keep to these rules, and one draw needn't show every extreme that they name: `documents`: document numbers never fall along the token order, start at 0, and each document has 1 to 256 tokens.
All inputs are finite; a program needn't handle non-finite values.
Results may differ from a plain program's by a relative error of at most 0.02.
Values may be sent and summed in bfloat16 or wider, within the bound.
A program may use at most 64 MiB of HBM per device.

v0:
```python
import jax
import jax.numpy as jnp
from jax import lax
from jax.sharding import PartitionSpec as P

HEAD_DIM = 64
WIN_ROWS = 8
WIN_COLS = 16
LAYERS = 3
GRID_W = 32
EPS = 1e-06


def with_halo(shard, sides, width, wrap):
    for axis, dim in sides:
        count, length = (lax.axis_size(axis), shard.shape[dim])
        up = [(i, (i + 1) % count) for i in range(count if wrap else count - 1)]
        down = [(j, i) for i, j in up]
        last = lax.slice_in_dim(shard, length - width, length, axis=dim)
        leading = lax.slice_in_dim(shard, 0, width, axis=dim)
        before = lax.ppermute(last, axis, up)
        after = lax.ppermute(leading, axis, down)
        shard = jnp.concatenate([before, shard, after], axis=dim)
    return shard


def rms_rows(stream, gain_row):
    values = stream.astype(jnp.float32)
    mean_sq = jnp.mean(values * values, axis=-1, keepdims=True)
    return (values * lax.rsqrt(mean_sq + EPS) * gain_row).astype(jnp.bfloat16)


def head_norm(heads_raw):
    values = heads_raw.astype(jnp.float32)
    mean_sq = jnp.mean(values * values, axis=-1, keepdims=True)
    return (values * lax.rsqrt(mean_sq + EPS)).astype(jnp.bfloat16)


def attend(queries, fringe, seg_own, seg_fringe, bias_layer):
    row_count, grid_width, head_count, head_width = queries.shape
    key_rows = jnp.stack(
        [fringe[row_lag : row_lag + row_count] for row_lag in range(WIN_ROWS)], axis=1
    )
    seg_rows = jnp.stack(
        [seg_fringe[row_lag : row_lag + row_count] for row_lag in range(WIN_ROWS)], axis=1
    )
    key_part = key_rows[..., :head_width]
    value_part = key_rows[..., head_width:]
    scores = jnp.einsum(
        "rchd,rjkhd->rhcjk", queries, key_part, preferred_element_type=jnp.float32
    ) * head_width ** (-0.5)
    column = jnp.arange(grid_width)
    col_offset = column[None, :] - column[:, None] + WIN_COLS // 2
    inside = (col_offset >= 0) & (col_offset < WIN_COLS)
    bias_table = bias_layer[:, :, jnp.clip(col_offset, 0, WIN_COLS - 1)]
    scores = scores + jnp.transpose(bias_table, (0, 2, 1, 3))[None]
    same_doc = seg_rows[:, None, None, :, :] == seg_own[:, None, :, None, None]
    allowed = same_doc & inside[None, None, :, None, :]
    scores = jnp.where(allowed, scores, -1e30)
    flat = scores.reshape(row_count, head_count, grid_width, WIN_ROWS * grid_width)
    attn_probs = jax.nn.softmax(flat, axis=-1).astype(jnp.bfloat16)
    attn_probs = attn_probs.reshape(row_count, head_count, grid_width, WIN_ROWS, grid_width)
    mixed_heads = jnp.einsum(
        "rhcjk,rjkhd->rchd", attn_probs, value_part, preferred_element_type=jnp.float32
    )
    return mixed_heads.astype(jnp.bfloat16)


def body(tokens, norm_gain, w_query, w_key, w_value, w_out, offset_bias, documents):
    token_count = tokens.shape[0]
    row_count = token_count // GRID_W
    reach_rows = WIN_ROWS // 2
    head_count = offset_bias.shape[1]
    seg_own = (documents + 1).reshape(row_count, GRID_W)
    seg_fringe = with_halo(seg_own, (("sp", 0),), reach_rows, False)
    collected = (
        lax.all_gather(w_query, "sp", axis=1, tiled=True),
        lax.all_gather(w_key, "sp", axis=1, tiled=True),
        lax.all_gather(w_value, "sp", axis=1, tiled=True),
        lax.all_gather(w_out, "sp", axis=2, tiled=True),
    )
    stream = tokens
    for layer_index in range(LAYERS):
        gathered = lax.all_gather(stream, "tp", axis=1, tiled=True)
        normed = rms_rows(gathered, norm_gain[layer_index])
        query_raw = jnp.dot(normed, collected[0][layer_index], preferred_element_type=jnp.float32)
        key_raw = jnp.dot(normed, collected[1][layer_index], preferred_element_type=jnp.float32)
        value_raw = jnp.dot(normed, collected[2][layer_index], preferred_element_type=jnp.float32)
        query_heads = head_norm(
            query_raw.astype(jnp.bfloat16).reshape(row_count, GRID_W, head_count, HEAD_DIM)
        )
        key_heads = head_norm(
            key_raw.astype(jnp.bfloat16).reshape(row_count, GRID_W, head_count, HEAD_DIM)
        )
        value_heads = value_raw.astype(jnp.bfloat16).reshape(
            row_count, GRID_W, head_count, HEAD_DIM
        )
        key_value = jnp.concatenate([key_heads, value_heads], axis=-1)
        fringe = with_halo(key_value, (("sp", 0),), reach_rows, False)
        attended = attend(query_heads, fringe, seg_own, seg_fringe, offset_bias[layer_index])
        attended = attended.reshape(token_count, head_count * HEAD_DIM)
        partial_sums = jnp.dot(
            attended, collected[3][layer_index], preferred_element_type=jnp.float32
        )
        stream = (
            lax.psum_scatter(
                partial_sums.astype(jnp.bfloat16), "tp", scatter_dimension=1, tiled=True
            )
            .astype(jnp.float32)
            .astype(jnp.bfloat16)
        )
    return stream


def solution(mesh):
    return jax.shard_map(
        body,
        mesh=mesh,
        in_specs=(
            P("sp", "tp"),
            P(),
            P(None, "sp", "tp"),
            P(None, "sp", "tp"),
            P(None, "sp", "tp"),
            P(None, "tp", "sp"),
            P(None, "tp", None, None),
            P("sp"),
        ),
        out_specs=P("sp", "tp"),
        check_vma=False,
    )
```

profile of v0, /device:TPU:0, one launch (start us, length us, event | category | flops | bytes accessed | tf_op | source)
XLA Modules:
  0.0 309.1 jit_solution(167499018848324964)
XLA Ops:
  9.5 4.9 %collective-permute-start.2 = (s32[4,32]{1,0:T(4,128)S(1)}, s32[4,32]{1,0:T(4,128)S(1)}, u32[]{:S(2)}, u32[]{:S(2)}) collective-permute-start(s32[4,32]{1,0:T(4,128)S(1)} %reshape.186), channel_id=1, source_target_pairs={{0,4},{4,8},{8,12},{12,16},{16,20},{20,24},{24,28},{1,5},{5,9},{9,... | collective-permute-start | bytes 1544 | tf_op jit(solution)/shard_map/ppermute | solution.py:21
  15.8 6.0 %all_gather.21 = bf16[128,1024]{1,0:T(8,128)(2,1)S(1)} all-gather(bf16[128,256]{1,0:T(8,128)(2,1)} %param.8), channel_id=1, replica_groups=mesh['sp'=8,'tp'=4] {'tp'}, dimensions={1}, use_global_device_ids=true | all-gather | bytes 327680 | tf_op jit(solution)/shard_map/all_gather | solution.py:84
  23.8 3.5 %gather_fusion = f32[1024,4,8]{2,1,0:T(4,128)S(1)} fusion(f32[4,8,16]{1,0,2:T(4,128)S(1)} %bitcast.251, s32[1024]{0:T(1024)S(1)} %broadcast_clamp_fusion), kind=kCustom, calls=%fused_computation | custom fusion | bytes 266240 | tf_op jit(solution)/shard_map/gather | solution.py:55
  29.0 27.4 %all-gather.5.cloned.1.call-done = bf16[3,1024,256]{2,1,0:T(8,128)(2,1)} async-done(((bf16[3,128,256]{2,1,0:T(8,128)(2,1)}), bf16[3,1024,256]{2,1,0:T(8,128)(2,1)}) %all-gather.5.cloned.1.call-update) | async-done | bytes 1572880 | tf_op jit(solution)/shard_map/all_gather | solution.py:78
  56.4 1.3 fusion.17
  58.4 42.8 %all-gather.7.cloned.1.call-done = bf16[3,1024,256]{2,1,0:T(8,128)(2,1)} async-done(((bf16[3,128,256]{2,1,0:T(8,128)(2,1)}), bf16[3,1024,256]{2,1,0:T(8,128)(2,1)}) %all-gather.7.cloned.1.call-update) | async-done | bytes 1572880 | tf_op jit(solution)/shard_map/all_gather | solution.py:79
  101.2 1.3 convolution_convert_fusion.10
  102.8 2.5 collective-permute-start
  106.5 39.4 %all-gather.9.cloned.1.call-done = bf16[3,1024,256]{2,1,0:T(8,128)(2,1)} async-done(((bf16[3,128,256]{2,1,0:T(8,128)(2,1)}), bf16[3,1024,256]{2,1,0:T(8,128)(2,1)}) %all-gather.9.cloned.1.call-update) | async-done | bytes 1572880 | tf_op jit(solution)/shard_map/all_gather | solution.py:77
  146.0 1.3 fusion.16
  150.8 39.8 %all-gather.11.cloned.1.call-done = bf16[3,256,1024]{2,1,0:T(8,128)(2,1)} async-done(((bf16[3,256,128]{2,1,0:T(8,128)(2,1)}), bf16[3,256,1024]{2,1,0:T(8,128)(2,1)}) %all-gather.11.cloned.1.call-update) | async-done | bytes 1572880 | tf_op jit(solution)/shard_map/all_gather | solution.py:80
  190.7 2.0 convolution_convert_fusion.2
  192.8 3.6 %gather_fusion.1 = f32[1024,4,8]{2,1,0:T(4,128)S(1)} fusion(f32[4,8,16]{1,0,2:T(4,128)S(1)} %bitcast.252, s32[1024]{0:T(1024)S(1)} %broadcast_clamp_fusion), kind=kCustom, calls=%fused_computation.1 | custom fusion | bytes 266240 | tf_op jit(solution)/shard_map/gather | solution.py:55
  197.6 13.6 %reduce-scatter.4.cloned.1.call-done = bf16[128,256]{1,0:T(8,128)(2,1)} async-done(((bf16[128,1024]{1,0:T(8,128)(2,1)}), bf16[128,256]{1,0:T(8,128)(2,1)}) %reduce-scatter.4.cloned.1.call-update) | async-done | bytes 65552 | tf_op jit(solution)/shard_map/reduce_scatter | solution.py:106
  211.2 6.0 %all_gather.26 = bf16[128,1024]{1,0:T(8,128)(2,1)S(1)} all-gather(bf16[128,256]{1,0:T(8,128)(2,1)} %reduce-scatter.4.cloned.1.call-done), channel_id=1, replica_groups=mesh['sp'=8,'tp'=4] {'tp'}, dimensions={1}, use_global_device_ids=true | all-gather | bytes 327680 | tf_op jit(solution)/shard_map/all_gather | solution.py:84
  217.4 1.3 fusion.15
  219.3 1.3 convolution_convert_fusion.7
  220.9 3.4 %collective-permute-start.4 = (bf16[4,32,4,128]{3,1,2,0:T(8,128)(2,1)S(1)}, bf16[4,32,4,128]{3,1,2,0:T(8,128)(2,1)S(1)}, u32[]{:S(2)}, u32[]{:S(2)}) collective-permute-start(bf16[4,32,4,128]{3,1,2,0:T(8,128)(2,1)S(1)} %pad_maximum_fusion.4), channel_id=1, source_target_pairs={{0,4},{4,8},{8,12},{12,16},{16,20},{20,24},{24,28},{1,5},{5,9},{9,... | collective-permute-start | bytes 393224 | tf_op jit(solution)/shard_map/ppermute | solution.py:21
  224.3 1.5 collective-permute-start.5
  225.8 1.3 fusion.14
  227.7 3.9 %collective-permute-done.5 = bf16[4,32,4,128]{3,1,2,0:T(8,128)(2,1)S(1)} collective-permute-done((bf16[4,32,4,128]{3,1,2,0:T(8,128)(2,1)S(1)}, bf16[4,32,4,128]{3,1,2,0:T(8,128)(2,1)S(1)}, u32[]{:S(2)}, u32[]{:S(2)}) %collective-permute-start.5) | collective-permute-done | bytes 131104 | tf_op jit(solution)/shard_map/ppermute | solution.py:22
  234.6 2.0 convolution_convert_fusion.1
  236.7 3.5 %gather_fusion.2 = f32[1024,4,8]{2,1,0:T(4,128)S(1)} fusion(f32[4,8,16]{1,0,2:T(4,128)S(1)} %bitcast.250, s32[1024]{0:T(1024)S(1)} %broadcast_clamp_fusion), kind=kCustom, calls=%fused_computation.2 | custom fusion | bytes 266240 | tf_op jit(solution)/shard_map/gather | solution.py:55
  241.5 15.2 %reduce-scatter.6.cloned.1.call-done = bf16[128,256]{1,0:T(8,128)(2,1)} async-done(((bf16[128,1024]{1,0:T(8,128)(2,1)}), bf16[128,256]{1,0:T(8,128)(2,1)}) %reduce-scatter.6.cloned.1.call-update) | async-done | bytes 65552 | tf_op jit(solution)/shard_map/reduce_scatter | solution.py:106
  256.7 6.0 %all_gather.27 = bf16[128,1024]{1,0:T(8,128)(2,1)S(1)} all-gather(bf16[128,256]{1,0:T(8,128)(2,1)} %reduce-scatter.6.cloned.1.call-done), channel_id=1, replica_groups=mesh['sp'=8,'tp'=4] {'tp'}, dimensions={1}, use_global_device_ids=true | all-gather | bytes 327680 | tf_op jit(solution)/shard_map/all_gather | solution.py:84
  262.9 1.3 fusion.13
  264.8 1.3 convolution_convert_fusion.4
  266.4 3.4 %collective-permute-start.6 = (bf16[4,32,4,128]{3,1,2,0:T(8,128)(2,1)S(1)}, bf16[4,32,4,128]{3,1,2,0:T(8,128)(2,1)S(1)}, u32[]{:S(2)}, u32[]{:S(2)}) collective-permute-start(bf16[4,32,4,128]{3,1,2,0:T(8,128)(2,1)S(1)} %pad_maximum_fusion.5), channel_id=1, source_target_pairs={{0,4},{4,8},{8,12},{12,16},{16,20},{20,24},{24,28},{1,5},{5,9},{9,... | collective-permute-start | bytes 393224 | tf_op jit(solution)/shard_map/ppermute | solution.py:21
  271.1 1.3 fusion.12
  273.1 4.1 %collective-permute-done.7 = bf16[4,32,4,128]{3,1,2,0:T(8,128)(2,1)S(1)} collective-permute-done((bf16[4,32,4,128]{3,1,2,0:T(8,128)(2,1)S(1)}, bf16[4,32,4,128]{3,1,2,0:T(8,128)(2,1)S(1)}, u32[]{:S(2)}, u32[]{:S(2)}) %collective-permute-start.7) | collective-permute-done | bytes 131104 | tf_op jit(solution)/shard_map/ppermute | solution.py:22
  280.1 2.0 convolution_convert_fusion
  282.1 20.2 %reduce-scatter.8.cloned.1.call-done = bf16[128,256]{1,0:T(8,128)(2,1)} async-done(((bf16[128,1024]{1,0:T(8,128)(2,1)}), bf16[128,256]{1,0:T(8,128)(2,1)}) %reduce-scatter.8.cloned.1.call-update) | async-done | bytes 65552 | tf_op jit(solution)/shard_map/reduce_scatter | solution.py:106
  (133 shorter events, 26.4 us)
Async XLA Ops:
  6.5 49.9 %all-gather.5.cloned.1.call-start = ((), (), s32[]{:S(2)}) async-start(), calls=%async_computation.3 | async-start | bytes 1769472 | tf_op jit(solution)/shard_map/all_gather | solution.py:78
  7.3 93.9 %all-gather.7.cloned.1.call-start = ((), (), s32[]{:S(2)}) async-start(), calls=%async_computation.4 | async-start | bytes 1769472 | tf_op jit(solution)/shard_map/all_gather | solution.py:79
  8.0 137.9 %all-gather.9.cloned.1.call-start = ((), (), s32[]{:S(2)}) async-start(), calls=%async_computation.5 | async-start | bytes 1769472 | tf_op jit(solution)/shard_map/all_gather | solution.py:77
  8.7 181.9 %all-gather.11.cloned.1.call-start = ((), (), s32[]{:S(2)}) async-start(), calls=%async_computation.6 | async-start | bytes 1769472 | tf_op jit(solution)/shard_map/all_gather | solution.py:80
  9.5 19.1 %collective-permute-start.2 = (s32[4,32]{1,0:T(4,128)S(1)}, s32[4,32]{1,0:T(4,128)S(1)}, u32[]{:S(2)}, u32[]{:S(2)}) collective-permute-start(s32[4,32]{1,0:T(4,128)S(1)} %reshape.186), channel_id=1, source_target_pairs={{0,4},{4,8},{8,12},{12,16},{16,20},{20,24},{24,28},{1,5},{5,9},{9,... | collective-permute-start | bytes 1544 | tf_op jit(solution)/shard_map/ppermute | solution.py:21
  14.4 14.2 %collective-permute-start.3 = (s32[4,32]{1,0:T(4,128)S(1)}, s32[4,32]{1,0:T(4,128)S(1)}, u32[]{:S(2)}, u32[]{:S(2)}) collective-permute-start(s32[4,32]{1,0:T(4,128)S(1)} %reshape.186), channel_id=1, source_target_pairs={{4,0},{8,4},{12,8},{16,12},{20,16},{24,20},{28,24},{5,1},{9,5},{13... | collective-permute-start | bytes 1544 | tf_op jit(solution)/shard_map/ppermute | solution.py:22
  15.7 195.5 %reduce-scatter.4.cloned.1.call-start = ((), (), s32[]{:S(2)}) async-start(), calls=%async_computation.7 | async-start | bytes 327680 | tf_op jit(solution)/shard_map/reduce_scatter | solution.py:106
  102.8 45.1 %collective-permute-start = (bf16[4,32,4,128]{3,1,2,0:T(8,128)(2,1)S(1)}, bf16[4,32,4,128]{3,1,2,0:T(8,128)(2,1)S(1)}, u32[]{:S(2)}, u32[]{:S(2)}) collective-permute-start(bf16[4,32,4,128]{3,1,2,0:T(8,128)(2,1)S(1)} %pad_maximum_fusion.3), channel_id=1, source_target_pairs={{0,4},{4,8},{8,12},{12,16},{16,20},{20,24},{24,28},{1,5},{5,9},{9,... | collective-permute-start | bytes 393224 | tf_op jit(solution)/shard_map/ppermute | solution.py:21
  105.2 42.7 %collective-permute-start.1 = (bf16[4,32,4,128]{3,1,2,0:T(8,128)(2,1)S(1)}, bf16[4,32,4,128]{3,1,2,0:T(8,128)(2,1)S(1)}, u32[]{:S(2)}, u32[]{:S(2)}) collective-permute-start(bf16[4,32,4,128]{3,1,2,0:T(8,128)(2,1)S(1)} %pad_maximum_fusion.3), channel_id=1, source_target_pairs={{4,0},{8,4},{12,8},{16,12},{20,16},{24,20},{28,24},{5,1},{9,5},{13... | collective-permute-start | bytes 393224 | tf_op jit(solution)/shard_map/ppermute | solution.py:22
  192.7 64.1 %reduce-scatter.6.cloned.1.call-start = ((), (), s32[]{:S(2)}) async-start(), calls=%async_computation.8 | async-start | bytes 327680 | tf_op jit(solution)/shard_map/reduce_scatter | solution.py:106
  220.9 6.8 %collective-permute-start.4 = (bf16[4,32,4,128]{3,1,2,0:T(8,128)(2,1)S(1)}, bf16[4,32,4,128]{3,1,2,0:T(8,128)(2,1)S(1)}, u32[]{:S(2)}, u32[]{:S(2)}) collective-permute-start(bf16[4,32,4,128]{3,1,2,0:T(8,128)(2,1)S(1)} %pad_maximum_fusion.4), channel_id=1, source_target_pairs={{0,4},{4,8},{8,12},{12,16},{16,20},{20,24},{24,28},{1,5},{5,9},{9,... | collective-permute-start | bytes 393224 | tf_op jit(solution)/shard_map/ppermute | solution.py:21
  224.3 7.4 %collective-permute-start.5 = (bf16[4,32,4,128]{3,1,2,0:T(8,128)(2,1)S(1)}, bf16[4,32,4,128]{3,1,2,0:T(8,128)(2,1)S(1)}, u32[]{:S(2)}, u32[]{:S(2)}) collective-permute-start(bf16[4,32,4,128]{3,1,2,0:T(8,128)(2,1)S(1)} %pad_maximum_fusion.4), channel_id=1, source_target_pairs={{4,0},{8,4},{12,8},{16,12},{20,16},{24,20},{28,24},{5,1},{9,5},{13... | collective-permute-start | bytes 393224 | tf_op jit(solution)/shard_map/ppermute | solution.py:22
  236.6 65.7 %reduce-scatter.8.cloned.1.call-start = ((), (), s32[]{:S(2)}) async-start(), calls=%async_computation.9 | async-start | bytes 327680 | tf_op jit(solution)/shard_map/reduce_scatter | solution.py:106
  266.4 6.6 %collective-permute-start.6 = (bf16[4,32,4,128]{3,1,2,0:T(8,128)(2,1)S(1)}, bf16[4,32,4,128]{3,1,2,0:T(8,128)(2,1)S(1)}, u32[]{:S(2)}, u32[]{:S(2)}) collective-permute-start(bf16[4,32,4,128]{3,1,2,0:T(8,128)(2,1)S(1)} %pad_maximum_fusion.5), channel_id=1, source_target_pairs={{0,4},{4,8},{8,12},{12,16},{16,20},{20,24},{24,28},{1,5},{5,9},{9,... | collective-permute-start | bytes 393224 | tf_op jit(solution)/shard_map/ppermute | solution.py:21
  269.8 7.4 %collective-permute-start.7 = (bf16[4,32,4,128]{3,1,2,0:T(8,128)(2,1)S(1)}, bf16[4,32,4,128]{3,1,2,0:T(8,128)(2,1)S(1)}, u32[]{:S(2)}, u32[]{:S(2)}) collective-permute-start(bf16[4,32,4,128]{3,1,2,0:T(8,128)(2,1)S(1)} %pad_maximum_fusion.5), channel_id=1, source_target_pairs={{4,0},{8,4},{12,8},{16,12},{20,16},{24,20},{28,24},{5,1},{9,5},{13... | collective-permute-start | bytes 393224 | tf_op jit(solution)/shard_map/ppermute | solution.py:22
Sparse Core Ops, SparseCore 0:
  9.5 46.8 all-gather.4
  58.6 42.5 all-gather.6
  103.4 42.5 all-gather.8
  147.8 42.7 all-gather.10
  193.0 18.2 reduce-scatter.3
  236.7 19.9 reduce-scatter.5
  282.2 20.0 reduce-scatter.7
where the time goes:
time: 310 us; the launch traced here: 309 us
  waiting for transfers between devices  209 us (67%)
  matrix products  23 us (7%)
  starting transfers between devices  19.7 us (6%)
  local copies, waits for them, and re-layouts  19.3 us (6%)
  blocking collectives  17.9 us (6%)
  between operations  14.2 us (5%)
  other arithmetic  6.3 us (2%)
    reduce_scatter x3, waiting for transfers between devices, body(): lax.psum_scatter(partial_sums.astype(jnp.bfloat16), 'tp', scatter_dimensi...  49 us
    all_gather x1, waiting for transfers between devices, body(): lax.all_gather(w_value, 'sp', axis=1, tiled=True)  42.8 us
    all_gather x1, waiting for transfers between devices, body(): lax.all_gather(w_out, 'sp', axis=2, tiled=True)  39.8 us
    all_gather x1, waiting for transfers between devices, body(): lax.all_gather(w_query, 'sp', axis=1, tiled=True)  39.4 us
    all_gather x1, waiting for transfers between devices, body(): lax.all_gather(w_key, 'sp', axis=1, tiled=True)  27.4 us
    all_gather x3, blocking collectives, body(): gathered = lax.all_gather(stream, 'tp', axis=1, tiled=True)  17.9 us
    gather x6, local copies, waits for them, and re-layouts, attend(): bias_table = bias_layer[:, :, jnp.clip(col_offset, 0, WIN_COLS - 1)]  14.4 us
    ppermute x4, starting transfers between devices, with_halo(): before = lax.ppermute(last, axis, up)  14.1 us
  transfers between devices with their start and end apart: 15, of which 9 were waited for; matrix products, arithmetic and copies ran while one was open for 10% of the time, Pallas kernels for 0%

commit v1 on v0

--- a/solution.py
+++ b/solution.py
@@ -1,3 +1,4 @@
+import functools
 import jax
 import jax.numpy as jnp
 from jax import lax
@@ -9,6 +10,31 @@
 LAYERS = 3
 GRID_W = 32
 EPS = 1e-06
+
+
+def move_the_frame(local, ax_name):
+    b_next = lax.psum(1, ax_name)
+    r1, finding, h_now = (b_next, lax.axis_index(ax_name), local.shape[2])
+    blocks_here = []
+    for ix, idx in enumerate(local.shape):
+        blocks_here.append(idx * r1 if ix == 2 else idx)
+    j0 = 1
+    then = lax.dynamic_update_slice_in_dim(
+        jnp.zeros(blocks_here, local.dtype), local, finding * h_now, axis=2
+    )
+    while j0 < r1:
+        stack_in = []
+        ix = 0
+        while ix < r1:
+            stack_in.append((ix, (ix + 1) % r1))
+            ix = ix + 1
+        local = lax.ppermute(local, ax_name, stack_in)
+        then = lax.dynamic_update_slice_in_dim(then, local, (finding - j0) % r1 * h_now, axis=2)
+        j0 = j0 + 1
+    return then
+
+
+_attach_knots = functools.partial(move_the_frame, ax_name="sp")
 
 
 def with_halo(shard, sides, width, wrap):
@@ -77,7 +103,7 @@
         lax.all_gather(w_query, "sp", axis=1, tiled=True),
         lax.all_gather(w_key, "sp", axis=1, tiled=True),
         lax.all_gather(w_value, "sp", axis=1, tiled=True),
-        lax.all_gather(w_out, "sp", axis=2, tiled=True),
+        _attach_knots(w_out),
     )
     stream = tokens
     for layer_index in range(LAYERS):

time: 310 us -> 279 us (0.900)
  waiting for transfers between devices: 209 us -> 158 us
  local copies, waits for them, and re-layouts: 19.3 us -> 36.6 us
  starting transfers between devices: 19.7 us -> 25 us
  matrix products: 23 us -> 19.9 us
    ppermute x0 -> x7, waiting for transfers between devices: none -> 65.3 us  [move_the_frame(): local = lax.ppermute(local, ax_name, stack_in)]
    all_gather x1 -> x0, waiting for transfers between devices: 39.8 us -> none  [body(): lax.all_gather(w_out, 'sp', axis=2, tiled=True)]
    all_gather x1, waiting for transfers between devices: 42.8 us -> 4.04 us  [body(): lax.all_gather(w_value, 'sp', axis=1, tiled=True)]
    all_gather x1, waiting for transfers between devices: 27.4 us -> 0.02 us  [body(): lax.all_gather(w_key, 'sp', axis=1, tiled=True)]
    gather x6, local copies, waits for them, and re-layouts: 14.4 us -> 31 us  [attend(): bias_table = bias_layer[:, :, jnp.clip(col_offset, 0, WIN_COLS - 1)]]
    reduce_scatter x3, waiting for transfers between devices: 49 us -> 38 us  [body(): lax.psum_scatter(partial_sums.astype(jnp.bfloat16), 'tp', scatter_dimensi...]
    ppermute x0 -> x7, starting transfers between devices: none -> 5.88 us  [move_the_frame(): local = lax.ppermute(local, ax_name, stack_in)]
    dot_general x3, matrix products: 5.97 us -> 2.84 us  [body(): jnp.dot(attended, collected[3][layer_index], preferred_element_type=jnp.f...]
  transfers between devices with their start and end apart: 15 -> 21, of which waited for: 9 -> 13; matrix products, arithmetic and copies ran while one was open for 10% -> 16% of each run, Pallas kernels for 0% -> 0%
where the time goes in v1:
time: 279 us; the launch traced here: 278 us
  waiting for transfers between devices  158 us (57%)
  local copies, waits for them, and re-layouts  36.6 us (13%)
  starting transfers between devices  25 us (9%)
  matrix products  19.9 us (7%)
  blocking collectives  17.9 us (6%)
  between operations  14.4 us (5%)
  other arithmetic  6.29 us (2%)
    ppermute x7, waiting for transfers between devices, move_the_frame(): local = lax.ppermute(local, ax_name, stack_in)  65.3 us
    all_gather x1, waiting for transfers between devices, body(): lax.all_gather(w_query, 'sp', axis=1, tiled=True)  40.8 us
    reduce_scatter x3, waiting for transfers between devices, body(): lax.psum_scatter(partial_sums.astype(jnp.bfloat16), 'tp', scatter_dimensi...  38 us
    gather x6, local copies, waits for them, and re-layouts, attend(): bias_table = bias_layer[:, :, jnp.clip(col_offset, 0, WIN_COLS - 1)]  31 us
    all_gather x3, blocking collectives, body(): gathered = lax.all_gather(stream, 'tp', axis=1, tiled=True)  17.9 us
    ppermute x4, starting transfers between devices, with_halo(): before = lax.ppermute(last, axis, up)  13.6 us
    ppermute x4, waiting for transfers between devices, with_halo(): after = lax.ppermute(leading, axis, down)  8.01 us
    ppermute x7, starting transfers between devices, move_the_frame(): local = lax.ppermute(local, ax_name, stack_in)  5.88 us
  transfers between devices with their start and end apart: 21, of which 13 were waited for; matrix products, arithmetic and copies ran while one was open for 16% of the time, Pallas kernels for 0%

profile of v1, /device:TPU:0, one launch (start us, length us, event | category | flops | bytes accessed | tf_op | source)
XLA Modules:
  0.0 277.8 jit_solution(13242562288782460515)
XLA Ops:
  8.8 4.9 %collective-permute-start.2 = (s32[4,32]{1,0:T(4,128)S(1)}, s32[4,32]{1,0:T(4,128)S(1)}, u32[]{:S(2)}, u32[]{:S(2)}) collective-permute-start(s32[4,32]{1,0:T(4,128)S(1)} %reshape.186), channel_id=1, source_target_pairs={{0,4},{4,8},{8,12},{12,16},{16,20},{20,24},{24,28},{1,5},{5,9},{9,... | collective-permute-start | bytes 1544 | tf_op jit(solution)/shard_map/ppermute | solution.py:47
  15.0 2.7 collective-permute-start.4
  18.0 6.0 %all_gather.18 = bf16[128,1024]{1,0:T(8,128)(2,1)S(1)} all-gather(bf16[128,256]{1,0:T(8,128)(2,1)} %param.8), channel_id=1, replica_groups=mesh['sp'=8,'tp'=4] {'tp'}, dimensions={1}, use_global_device_ids=true | all-gather | bytes 327680 | tf_op jit(solution)/shard_map/all_gather | solution.py:110
  26.2 7.9 %gather_fusion = f32[1024,4,8]{2,1,0:T(4,128)} fusion(f32[4,8,16]{1,0,2:T(4,128)S(1)} %bitcast.250, s32[1024]{0:T(1024)S(1)} %broadcast_clamp_fusion), kind=kCustom, calls=%fused_computation | custom fusion | bytes 266240 | tf_op jit(solution)/shard_map/gather | solution.py:81
  34.1 2.4 copy.150
  36.7 2.5 collective-permute-start.5
  39.2 11.1 %collective-permute-done.5 = bf16[3,256,128]{2,1,0:T(8,128)(2,1)S(1)} collective-permute-done((bf16[3,256,128]{2,1,0:T(8,128)(2,1)S(1)}, bf16[3,256,128]{2,1,0:T(8,128)(2,1)S(1)}, u32[]{:S(2)}, u32[]{:S(2)}) %collective-permute-start.5) | collective-permute-done | bytes 196640 | tf_op jit(solution)/shard_map/ppermute | solution.py:31
  50.9 12.1 %collective-permute-done.6 = bf16[3,256,128]{2,1,0:T(8,128)(2,1)S(1)} collective-permute-done((bf16[3,256,128]{2,1,0:T(8,128)(2,1)S(1)}, bf16[3,256,128]{2,1,0:T(8,128)(2,1)S(1)}, u32[]{:S(2)}, u32[]{:S(2)}) %collective-permute-start.6) | collective-permute-done | bytes 196640 | tf_op jit(solution)/shard_map/ppermute | solution.py:31
  63.3 8.2 %collective-permute-done.7 = bf16[3,256,128]{2,1,0:T(8,128)(2,1)S(1)} collective-permute-done((bf16[3,256,128]{2,1,0:T(8,128)(2,1)S(1)}, bf16[3,256,128]{2,1,0:T(8,128)(2,1)S(1)}, u32[]{:S(2)}, u32[]{:S(2)}) %collective-permute-start.7) | collective-permute-done | bytes 196640 | tf_op jit(solution)/shard_map/ppermute | solution.py:31
  71.6 13.2 %collective-permute-done.8 = bf16[3,256,128]{2,1,0:T(8,128)(2,1)S(1)} collective-permute-done((bf16[3,256,128]{2,1,0:T(8,128)(2,1)S(1)}, bf16[3,256,128]{2,1,0:T(8,128)(2,1)S(1)}, u32[]{:S(2)}, u32[]{:S(2)}) %collective-permute-start.8) | collective-permute-done | bytes 196640 | tf_op jit(solution)/shard_map/ppermute | solution.py:31
  85.0 8.6 %collective-permute-done.9 = bf16[3,256,128]{2,1,0:T(8,128)(2,1)S(1)} collective-permute-done((bf16[3,256,128]{2,1,0:T(8,128)(2,1)S(1)}, bf16[3,256,128]{2,1,0:T(8,128)(2,1)S(1)}, u32[]{:S(2)}, u32[]{:S(2)}) %collective-permute-start.9) | collective-permute-done | bytes 196640 | tf_op jit(solution)/shard_map/ppermute | solution.py:31
  93.7 12.1 %collective-permute-done.10 = bf16[3,256,128]{2,1,0:T(8,128)(2,1)S(1)} collective-permute-done((bf16[3,256,128]{2,1,0:T(8,128)(2,1)S(1)}, bf16[3,256,128]{2,1,0:T(8,128)(2,1)S(1)}, u32[]{:S(2)}, u32[]{:S(2)}) %collective-permute-start.10) | collective-permute-done | bytes 196640 | tf_op jit(solution)/shard_map/ppermute | solution.py:31
  105.9 1.3 fusion.17
  107.7 4.0 %all-gather.6.cloned.1.call-done = bf16[3,1024,256]{2,1,0:T(8,128)(2,1)} async-done(((bf16[3,128,256]{2,1,0:T(8,128)(2,1)}), bf16[3,1024,256]{2,1,0:T(8,128)(2,1)}) %all-gather.6.cloned.1.call-update) | async-done | bytes 1572880 | tf_op jit(solution)/shard_map/all_gather | solution.py:105
  113.5 1.9 collective-permute-start
  116.7 40.8 %all-gather.8.cloned.1.call-done = bf16[3,1024,256]{2,1,0:T(8,128)(2,1)} async-done(((bf16[3,128,256]{2,1,0:T(8,128)(2,1)}), bf16[3,1024,256]{2,1,0:T(8,128)(2,1)}) %all-gather.8.cloned.1.call-update) | async-done | bytes 1572880 | tf_op jit(solution)/shard_map/all_gather | solution.py:103
  163.5 8.0 %gather_fusion.1 = f32[1024,4,8]{2,1,0:T(4,128)} fusion(f32[4,8,16]{1,0,2:T(4,128)S(1)} %bitcast.252, s32[1024]{0:T(1024)S(1)} %broadcast_clamp_fusion), kind=kCustom, calls=%fused_computation.1 | custom fusion | bytes 266240 | tf_op jit(solution)/shard_map/gather | solution.py:81
  171.5 2.4 copy.167
  173.9 8.1 %reduce-scatter.4.cloned.1.call-done = bf16[128,256]{1,0:T(8,128)(2,1)} async-done(((bf16[128,1024]{1,0:T(8,128)(2,1)}), bf16[128,256]{1,0:T(8,128)(2,1)}) %reduce-scatter.4.cloned.1.call-update) | async-done | bytes 65552 | tf_op jit(solution)/shard_map/reduce_scatter | solution.py:132
  182.0 6.0 %all_gather.22 = bf16[128,1024]{1,0:T(8,128)(2,1)S(1)} all-gather(bf16[128,256]{1,0:T(8,128)(2,1)} %reduce-scatter.4.cloned.1.call-done), channel_id=1, replica_groups=mesh['sp'=8,'tp'=4] {'tp'}, dimensions={1}, use_global_device_ids=true | all-gather | bytes 327680 | tf_op jit(solution)/shard_map/all_gather | solution.py:110
  188.1 1.3 fusion.15
  190.1 1.3 convolution_convert_fusion.7
  191.7 3.4 %collective-permute-start.11 = (bf16[4,32,4,128]{3,1,2,0:T(8,128)(2,1)S(1)}, bf16[4,32,4,128]{3,1,2,0:T(8,128)(2,1)S(1)}, u32[]{:S(2)}, u32[]{:S(2)}) collective-permute-start(bf16[4,32,4,128]{3,1,2,0:T(8,128)(2,1)S(1)} %pad_maximum_fusion.4), channel_id=1, source_target_pairs={{0,4},{4,8},{8,12},{12,16},{16,20},{20,24},{24,28},{1,5},{5,9},{9,... | collective-permute-start | bytes 393224 | tf_op jit(solution)/shard_map/ppermute | solution.py:47
  195.1 1.5 collective-permute-start.12
  198.5 3.9 %collective-permute-done.12 = bf16[4,32,4,128]{3,1,2,0:T(8,128)(2,1)S(1)} collective-permute-done((bf16[4,32,4,128]{3,1,2,0:T(8,128)(2,1)S(1)}, bf16[4,32,4,128]{3,1,2,0:T(8,128)(2,1)S(1)}, u32[]{:S(2)}, u32[]{:S(2)}) %collective-permute-start.12) | collective-permute-done | bytes 131104 | tf_op jit(solution)/shard_map/ppermute | solution.py:48
  206.4 8.0 %gather_fusion.2 = f32[1024,4,8]{2,1,0:T(4,128)} fusion(f32[4,8,16]{1,0,2:T(4,128)S(1)} %bitcast.251, s32[1024]{0:T(1024)S(1)} %broadcast_clamp_fusion), kind=kCustom, calls=%fused_computation.2 | custom fusion | bytes 266240 | tf_op jit(solution)/shard_map/gather | solution.py:81
  214.4 2.4 copy.184
  216.8 9.7 %reduce-scatter.6.cloned.1.call-done = bf16[128,256]{1,0:T(8,128)(2,1)} async-done(((bf16[128,1024]{1,0:T(8,128)(2,1)}), bf16[128,256]{1,0:T(8,128)(2,1)}) %reduce-scatter.6.cloned.1.call-update) | async-done | bytes 65552 | tf_op jit(solution)/shard_map/reduce_scatter | solution.py:132
  226.5 6.0 %all_gather.23 = bf16[128,1024]{1,0:T(8,128)(2,1)S(1)} all-gather(bf16[128,256]{1,0:T(8,128)(2,1)} %reduce-scatter.6.cloned.1.call-done), channel_id=1, replica_groups=mesh['sp'=8,'tp'=4] {'tp'}, dimensions={1}, use_global_device_ids=true | all-gather | bytes 327680 | tf_op jit(solution)/shard_map/all_gather | solution.py:110
  236.2 3.4 %collective-permute-start.13 = (bf16[4,32,4,128]{3,1,2,0:T(8,128)(2,1)S(1)}, bf16[4,32,4,128]{3,1,2,0:T(8,128)(2,1)S(1)}, u32[]{:S(2)}, u32[]{:S(2)}) collective-permute-start(bf16[4,32,4,128]{3,1,2,0:T(8,128)(2,1)S(1)} %pad_maximum_fusion.5), channel_id=1, source_target_pairs={{0,4},{4,8},{8,12},{12,16},{16,20},{20,24},{24,28},{1,5},{5,9},{9,... | collective-permute-start | bytes 393224 | tf_op jit(solution)/shard_map/ppermute | solution.py:47
  242.8 4.1 %collective-permute-done.14 = bf16[4,32,4,128]{3,1,2,0:T(8,128)(2,1)S(1)} collective-permute-done((bf16[4,32,4,128]{3,1,2,0:T(8,128)(2,1)S(1)}, bf16[4,32,4,128]{3,1,2,0:T(8,128)(2,1)S(1)}, u32[]{:S(2)}, u32[]{:S(2)}) %collective-permute-start.14) | collective-permute-done | bytes 131104 | tf_op jit(solution)/shard_map/ppermute | solution.py:48
  250.8 20.2 %reduce-scatter.8.cloned.1.call-done = bf16[128,256]{1,0:T(8,128)(2,1)} async-done(((bf16[128,1024]{1,0:T(8,128)(2,1)}), bf16[128,256]{1,0:T(8,128)(2,1)}) %reduce-scatter.8.cloned.1.call-update) | async-done | bytes 65552 | tf_op jit(solution)/shard_map/reduce_scatter | solution.py:132
  (155 shorter events, 34.1 us)
Async XLA Ops:
  6.5 19.6 %copy-start = (bf16[3,256,128]{2,1,0:T(8,128)(2,1)S(1)}, bf16[3,256,128]{2,1,0:T(8,128)(2,1)}, u32[]{:S(2)}) copy-start(bf16[3,256,128]{2,1,0:T(8,128)(2,1)} %param.13) | copy-start | bytes 589828
  6.5 99.3 %all-gather.4.cloned.1.call-start = ((), (), s32[]{:S(2)}) async-start(), calls=%async_computation.3 | async-start | bytes 1769472 | tf_op jit(solution)/shard_map/all_gather | solution.py:104
  7.3 104.5 %all-gather.6.cloned.1.call-start = ((), (), s32[]{:S(2)}) async-start(), calls=%async_computation.4 | async-start | bytes 1769472 | tf_op jit(solution)/shard_map/all_gather | solution.py:105
  8.0 149.5 %all-gather.8.cloned.1.call-start = ((), (), s32[]{:S(2)}) async-start(), calls=%async_computation.5 | async-start | bytes 1769472 | tf_op jit(solution)/shard_map/all_gather | solution.py:103
  8.8 27.7 %collective-permute-start.2 = (s32[4,32]{1,0:T(4,128)S(1)}, s32[4,32]{1,0:T(4,128)S(1)}, u32[]{:S(2)}, u32[]{:S(2)}) collective-permute-start(s32[4,32]{1,0:T(4,128)S(1)} %reshape.186), channel_id=1, source_target_pairs={{0,4},{4,8},{8,12},{12,16},{16,20},{20,24},{24,28},{1,5},{5,9},{9,... | collective-permute-start | bytes 1544 | tf_op jit(solution)/shard_map/ppermute | solution.py:47
  13.7 22.9 %collective-permute-start.3 = (s32[4,32]{1,0:T(4,128)S(1)}, s32[4,32]{1,0:T(4,128)S(1)}, u32[]{:S(2)}, u32[]{:S(2)}) collective-permute-start(s32[4,32]{1,0:T(4,128)S(1)} %reshape.186), channel_id=1, source_target_pairs={{4,0},{8,4},{12,8},{16,12},{20,16},{24,20},{28,24},{5,1},{9,5},{13... | collective-permute-start | bytes 1544 | tf_op jit(solution)/shard_map/ppermute | solution.py:48
  15.0 21.7 %collective-permute-start.4 = (bf16[3,256,128]{2,1,0:T(8,128)(2,1)}, bf16[3,256,128]{2,1,0:T(8,128)(2,1)S(1)}, u32[]{:S(2)}, u32[]{:S(2)}) collective-permute-start(bf16[3,256,128]{2,1,0:T(8,128)(2,1)} %param.13), channel_id=1, source_target_pairs={{0,4},{4,8},{8,12},{12,16},{16,20},{20,24},{24,28},{28,0},{1,5},{5... | collective-permute-start | bytes 589832 | tf_op jit(solution)/shard_map/ppermute | solution.py:31
  17.7 164.3 %reduce-scatter.4.cloned.1.call-start = ((), (), s32[]{:S(2)}) async-start(), calls=%async_computation.6 | async-start | bytes 327680 | tf_op jit(solution)/shard_map/reduce_scatter | solution.py:132
  36.7 13.6 %collective-permute-start.5 = (bf16[3,256,128]{2,1,0:T(8,128)(2,1)S(1)}, bf16[3,256,128]{2,1,0:T(8,128)(2,1)S(1)}, u32[]{:S(2)}, u32[]{:S(2)}) collective-permute-start(bf16[3,256,128]{2,1,0:T(8,128)(2,1)S(1)} %collective-permute-done.4), channel_id=1, source_target_pairs={{0,4},{4,8},{8,12},{12,16},{16,20},{20,24},{24,28},{28,0},{1,5},{5... | collective-permute-start | bytes 589832 | tf_op jit(solution)/shard_map/ppermute | solution.py:31
  50.2 12.8 %collective-permute-start.6 = (bf16[3,256,128]{2,1,0:T(8,128)(2,1)S(1)}, bf16[3,256,128]{2,1,0:T(8,128)(2,1)S(1)}, u32[]{:S(2)}, u32[]{:S(2)}) collective-permute-start(bf16[3,256,128]{2,1,0:T(8,128)(2,1)S(1)} %collective-permute-done.5), channel_id=1, source_target_pairs={{0,4},{4,8},{8,12},{12,16},{16,20},{20,24},{24,28},{28,0},{1,5},{5... | collective-permute-start | bytes 589832 | tf_op jit(solution)/shard_map/ppermute | solution.py:31
  63.1 8.4 %collective-permute-start.7 = (bf16[3,256,128]{2,1,0:T(8,128)(2,1)S(1)}, bf16[3,256,128]{2,1,0:T(8,128)(2,1)S(1)}, u32[]{:S(2)}, u32[]{:S(2)}) collective-permute-start(bf16[3,256,128]{2,1,0:T(8,128)(2,1)S(1)} %collective-permute-done.6), channel_id=1, source_target_pairs={{0,4},{4,8},{8,12},{12,16},{16,20},{20,24},{24,28},{28,0},{1,5},{5... | collective-permute-start | bytes 589832 | tf_op jit(solution)/shard_map/ppermute | solution.py:31
  71.4 13.4 %collective-permute-start.8 = (bf16[3,256,128]{2,1,0:T(8,128)(2,1)S(1)}, bf16[3,256,128]{2,1,0:T(8,128)(2,1)S(1)}, u32[]{:S(2)}, u32[]{:S(2)}) collective-permute-start(bf16[3,256,128]{2,1,0:T(8,128)(2,1)S(1)} %collective-permute-done.7), channel_id=1, source_target_pairs={{0,4},{4,8},{8,12},{12,16},{16,20},{20,24},{24,28},{28,0},{1,5},{5... | collective-permute-start | bytes 589832 | tf_op jit(solution)/shard_map/ppermute | solution.py:31
  84.8 8.8 %collective-permute-start.9 = (bf16[3,256,128]{2,1,0:T(8,128)(2,1)S(1)}, bf16[3,256,128]{2,1,0:T(8,128)(2,1)S(1)}, u32[]{:S(2)}, u32[]{:S(2)}) collective-permute-start(bf16[3,256,128]{2,1,0:T(8,128)(2,1)S(1)} %collective-permute-done.8), channel_id=1, source_target_pairs={{0,4},{4,8},{8,12},{12,16},{16,20},{20,24},{24,28},{28,0},{1,5},{5... | collective-permute-start | bytes 589832 | tf_op jit(solution)/shard_map/ppermute | solution.py:31
  93.6 12.2 %collective-permute-start.10 = (bf16[3,256,128]{2,1,0:T(8,128)(2,1)S(1)}, bf16[3,256,128]{2,1,0:T(8,128)(2,1)S(1)}, u32[]{:S(2)}, u32[]{:S(2)}) collective-permute-start(bf16[3,256,128]{2,1,0:T(8,128)(2,1)S(1)} %collective-permute-done.9), channel_id=1, source_target_pairs={{0,4},{4,8},{8,12},{12,16},{16,20},{20,24},{24,28},{28,0},{1,5},{5... | collective-permute-start | bytes 589832 | tf_op jit(solution)/shard_map/ppermute | solution.py:31
  113.5 46.0 %collective-permute-start = (bf16[4,32,4,128]{3,1,2,0:T(8,128)(2,1)S(1)}, bf16[4,32,4,128]{3,1,2,0:T(8,128)(2,1)S(1)}, u32[]{:S(2)}, u32[]{:S(2)}) collective-permute-start(bf16[4,32,4,128]{3,1,2,0:T(8,128)(2,1)S(1)} %pad_maximum_fusion.3), channel_id=1, source_target_pairs={{0,4},{4,8},{8,12},{12,16},{16,20},{20,24},{24,28},{1,5},{5,9},{9,... | collective-permute-start | bytes 393224 | tf_op jit(solution)/shard_map/ppermute | solution.py:47
  115.4 44.1 %collective-permute-start.1 = (bf16[4,32,4,128]{3,1,2,0:T(8,128)(2,1)S(1)}, bf16[4,32,4,128]{3,1,2,0:T(8,128)(2,1)S(1)}, u32[]{:S(2)}, u32[]{:S(2)}) collective-permute-start(bf16[4,32,4,128]{3,1,2,0:T(8,128)(2,1)S(1)} %pad_maximum_fusion.3), channel_id=1, source_target_pairs={{4,0},{8,4},{12,8},{16,12},{20,16},{24,20},{28,24},{5,1},{9,5},{13... | collective-permute-start | bytes 393224 | tf_op jit(solution)/shard_map/ppermute | solution.py:48
  163.4 63.1 %reduce-scatter.6.cloned.1.call-start = ((), (), s32[]{:S(2)}) async-start(), calls=%async_computation.7 | async-start | bytes 327680 | tf_op jit(solution)/shard_map/reduce_scatter | solution.py:132
  191.7 6.8 %collective-permute-start.11 = (bf16[4,32,4,128]{3,1,2,0:T(8,128)(2,1)S(1)}, bf16[4,32,4,128]{3,1,2,0:T(8,128)(2,1)S(1)}, u32[]{:S(2)}, u32[]{:S(2)}) collective-permute-start(bf16[4,32,4,128]{3,1,2,0:T(8,128)(2,1)S(1)} %pad_maximum_fusion.4), channel_id=1, source_target_pairs={{0,4},{4,8},{8,12},{12,16},{16,20},{20,24},{24,28},{1,5},{5,9},{9,... | collective-permute-start | bytes 393224 | tf_op jit(solution)/shard_map/ppermute | solution.py:47
  195.1 7.4 %collective-permute-start.12 = (bf16[4,32,4,128]{3,1,2,0:T(8,128)(2,1)S(1)}, bf16[4,32,4,128]{3,1,2,0:T(8,128)(2,1)S(1)}, u32[]{:S(2)}, u32[]{:S(2)}) collective-permute-start(bf16[4,32,4,128]{3,1,2,0:T(8,128)(2,1)S(1)} %pad_maximum_fusion.4), channel_id=1, source_target_pairs={{4,0},{8,4},{12,8},{16,12},{20,16},{24,20},{28,24},{5,1},{9,5},{13... | collective-permute-start | bytes 393224 | tf_op jit(solution)/shard_map/ppermute | solution.py:48
  206.3 64.7 %reduce-scatter.8.cloned.1.call-start = ((), (), s32[]{:S(2)}) async-start(), calls=%async_computation.8 | async-start | bytes 327680 | tf_op jit(solution)/shard_map/reduce_scatter | solution.py:132
  236.2 6.6 %collective-permute-start.13 = (bf16[4,32,4,128]{3,1,2,0:T(8,128)(2,1)S(1)}, bf16[4,32,4,128]{3,1,2,0:T(8,128)(2,1)S(1)}, u32[]{:S(2)}, u32[]{:S(2)}) collective-permute-start(bf16[4,32,4,128]{3,1,2,0:T(8,128)(2,1)S(1)} %pad_maximum_fusion.5), channel_id=1, source_target_pairs={{0,4},{4,8},{8,12},{12,16},{16,20},{20,24},{24,28},{1,5},{5,9},{9,... | collective-permute-start | bytes 393224 | tf_op jit(solution)/shard_map/ppermute | solution.py:47
  239.6 7.4 %collective-permute-start.14 = (bf16[4,32,4,128]{3,1,2,0:T(8,128)(2,1)S(1)}, bf16[4,32,4,128]{3,1,2,0:T(8,128)(2,1)S(1)}, u32[]{:S(2)}, u32[]{:S(2)}) collective-permute-start(bf16[4,32,4,128]{3,1,2,0:T(8,128)(2,1)S(1)} %pad_maximum_fusion.5), channel_id=1, source_target_pairs={{4,0},{8,4},{12,8},{16,12},{20,16},{24,20},{28,24},{5,1},{9,5},{13... | collective-permute-start | bytes 393224 | tf_op jit(solution)/shard_map/ppermute | solution.py:48
Sparse Core Ops, SparseCore 0:
  9.5 52.0 all-gather.3
  63.8 47.9 all-gather.5
  113.9 43.5 all-gather.7
  163.5 18.4 reduce-scatter.3
  206.4 20.0 reduce-scatter.5
  250.9 20.0 reduce-scatter.7
